TPU v7x, 32 devices: a whole 2x2x4 slice. The times are simulated.
32 devices in a mesh: fs: 8 (over z, y), tp: 4 (over x, core).
Axes of the slice: x: 2, y: 2, z: 4, core: 2. Of those that a mesh axis runs over, the one named last changes fastest.
Arguments:
- tokens: bfloat16 [640, 3072], P('tp'), may hold values from -6 to 6
- gain_first: float32 [3072], replicated, may hold values from 0.1 to 1.9
- gain_second: float32 [3072], replicated, may hold values from 0.1 to 1.9
- gate_first: float32 [3072, 8192], P('fs', 'tp'), may hold values from -0.109375 to 0.109375
- up_first: float32 [3072, 8192], P('fs', 'tp'), may hold values from -0.109375 to 0.109375
- down_first: float32 [8192, 3072], P('fs', 'tp'), may hold values from -0.09375 to 0.09375
- gate_second: float32 [3072, 8192], P('fs', 'tp'), may hold values from -0.109375 to 0.109375
- up_second: float32 [3072, 8192], P('fs', 'tp'), may hold values from -0.109375 to 0.109375
- down_second: float32 [8192, 3072], P('fs', 'tp'), may hold values from -0.09375 to 0.09375
Outputs:
- result_rows: bfloat16 [640, 3072], P('tp')
- serve_gate_first: bfloat16 [3072, 8192], P(None, 'fs')
- serve_up_first: bfloat16 [3072, 8192], P(None, 'fs')
- serve_down_first: bfloat16 [8192, 3072], P('fs')
- serve_gate_second: bfloat16 [3072, 8192], P(None, 'fs')
- serve_up_second: bfloat16 [3072, 8192], P(None, 'fs')
- serve_down_second: bfloat16 [8192, 3072], P('fs')
All inputs are finite; a program needn't handle non-finite values.
Results may differ from a plain program's by a relative error of at most 0.011.
Values may be sent and summed in bfloat16 or wider, within the bound.
A program may use at most 192 MiB of HBM per device.

v0:
```python
import jax
import jax.numpy as jnp
from jax import lax
from jax.sharding import PartitionSpec as P


def plain_norm(values):
    values = values.astype(jnp.float32)
    center = jnp.mean(values, axis=-1, keepdims=True)
    spread = jnp.mean(jnp.square(values - center), axis=-1, keepdims=True)
    return (values - center) * lax.rsqrt(spread + 1e-05)


def half_step(normed, scales, w_gate, w_rising, w_down):
    gate_part = jnp.dot(normed, w_gate, preferred_element_type=jnp.float32)
    rising = jnp.dot(normed, w_rising, preferred_element_type=jnp.float32)
    hidden = (jax.nn.silu(gate_part) * rising).astype(jnp.bfloat16)
    partial_value = jnp.dot(hidden, w_down, preferred_element_type=jnp.float32)
    block = lax.psum(partial_value, "fs")
    mixed = 1.6817928 * scales[None, :] * normed.astype(jnp.float32) + 0.5 * block
    return plain_norm(mixed).astype(jnp.bfloat16)


def on_device(
    tokens,
    gain_first,
    gain_second,
    gate_first,
    up_first,
    down_first,
    gate_second,
    up_second,
    down_second,
):
    row_count = gate_first.shape[0]
    offset = lax.axis_index("fs") * row_count

    def fold_gain(weight, scales):
        picked = lax.dynamic_slice_in_dim(scales, offset, row_count, 0)
        return (picked[:, None] * weight).astype(jnp.bfloat16)

    widened = (
        lax.all_gather(fold_gain(gate_first, gain_first), "tp", axis=1, tiled=True),
        lax.all_gather(fold_gain(up_first, gain_first), "tp", axis=1, tiled=True),
        lax.all_gather(fold_gain(gate_second, gain_second), "tp", axis=1, tiled=True),
        lax.all_gather(fold_gain(up_second, gain_second), "tp", axis=1, tiled=True),
        lax.all_gather(down_first.astype(jnp.bfloat16), "tp", axis=1, tiled=True),
        lax.all_gather(down_second.astype(jnp.bfloat16), "tp", axis=1, tiled=True),
    )
    regrouped = (
        lax.all_to_all(widened[0], "fs", split_axis=1, concat_axis=0, tiled=True),
        lax.all_to_all(widened[1], "fs", split_axis=1, concat_axis=0, tiled=True),
        lax.all_to_all(widened[2], "fs", split_axis=1, concat_axis=0, tiled=True),
        lax.all_to_all(widened[3], "fs", split_axis=1, concat_axis=0, tiled=True),
    )
    serve_gate_first, serve_up_first, serve_gate_second, serve_up_second = regrouped
    serve_down_first = widened[4]
    serve_down_second = widened[5]
    normed_zero = plain_norm(tokens).astype(jnp.bfloat16)
    normed_one = half_step(
        normed_zero, gain_first, serve_gate_first, serve_up_first, serve_down_first
    )
    result_rows = half_step(
        normed_one, gain_second, serve_gate_second, serve_up_second, serve_down_second
    )
    return (
        result_rows,
        serve_gate_first,
        serve_up_first,
        serve_down_first,
        serve_gate_second,
        serve_up_second,
        serve_down_second,
    )


def solution(mesh):
    placed = (
        P("tp", None),
        P(),
        P(),
        P("fs", "tp"),
        P("fs", "tp"),
        P("fs", "tp"),
        P("fs", "tp"),
        P("fs", "tp"),
        P("fs", "tp"),
    )
    return jax.shard_map(
        on_device,
        mesh=mesh,
        in_specs=placed,
        out_specs=(
            P("tp", None),
            P(None, "fs"),
            P(None, "fs"),
            P("fs", None),
            P(None, "fs"),
            P(None, "fs"),
            P("fs", None),
        ),
        check_vma=False,
    )
```

profile of v0, /device:TPU:0, one launch (start us, length us, event | category | flops | bytes accessed | tf_op | source)
XLA Modules:
  0.0 865.7 jit_solution(17595812001735718184)
XLA Ops:
  8.0 5.5 multiply_convert_fusion.3
  14.3 48.5 %all-gather.7.cloned.1.call-done = bf16[384,8192]{1,0:T(8,128)(2,1)} async-done(((bf16[384,2048]{1,0:T(8,128)(2,1)}), bf16[384,8192]{1,0:T(8,128)(2,1)}) %all-gather.7.cloned.1.call-update) | async-done | bytes 6291472 | tf_op jit(solution)/shard_map/all_gather | solution.py:43
  62.7 6.5 copy.31
  69.2 5.8 all-to-all-start
  75.2 4.7 multiply_convert_fusion.1
  79.9 31.4 %all-gather.9.cloned.1.call-done = bf16[384,8192]{1,0:T(8,128)(2,1)} async-done(((bf16[384,2048]{1,0:T(8,128)(2,1)}), bf16[384,8192]{1,0:T(8,128)(2,1)}) %all-gather.9.cloned.1.call-update) | async-done | bytes 6291472 | tf_op jit(solution)/shard_map/all_gather | solution.py:44
  111.3 6.5 copy.30
  117.8 95.9 %all-to-all-done = bf16[384,8,1024]{2,0,1:T(8,128)(2,1)} async-done(((bf16[384,8,1024]{2,0,1:T(8,128)(2,1)}), bf16[384,8,1024]{2,0,1:T(8,128)(2,1)}, u32[]{:S(2)}, u32[]{:S(2)}) %all-to-all-start) | async-done | bytes 6291488 | tf_op jit(solution)/shard_map/all_to_all | solution.py:51
  213.7 5.0 all-to-all-start.1
  220.1 6.5 copy.29
  226.6 129.8 %all-to-all-done.1 = bf16[384,8,1024]{2,0,1:T(8,128)(2,1)} async-done(((bf16[384,8,1024]{2,0,1:T(8,128)(2,1)}), bf16[384,8,1024]{2,0,1:T(8,128)(2,1)}, u32[]{:S(2)}, u32[]{:S(2)}) %all-to-all-start.1) | async-done | bytes 6291488 | tf_op jit(solution)/shard_map/all_to_all | solution.py:52
  356.4 4.8 all-to-all-start.2
  363.0 4.0 fusion.16
  367.1 8.9 %fusion.7 = f32[160,3072]{1,0:T(8,128)} fusion(bf16[1024,3072]{1,0:T(8,128)(2,1)} %all-gather.11.cloned.1.call-done, bf16[3072,1024]{1,0:T(8,128)(2,1)} %bitcast.3, f32[160,1024]{1,0:T(8,128)S(1)} %fusion.16, bf16[160,3072]{1,0:T(8,128)(2,1)S(1)} %copy-done, f32[160]{0:T(256)S(1)} %add_rsqrt_fusion.2, f32[160]{0:T(256)S(1)} %broadcast_multiply_fusion.4), kind=kOutput, calls=%fused_computation.25 | convolution fusion | flops 2016215040 | bytes 16188672 | tf_op jit(solution)/shard_map/dot_general | solution.py:18
  376.0 34.6 %all-gather.15.cloned.1.call-done = bf16[384,8192]{1,0:T(8,128)(2,1)} async-done(((bf16[384,2048]{1,0:T(8,128)(2,1)}), bf16[384,8192]{1,0:T(8,128)(2,1)}) %all-gather.15.cloned.1.call-update) | async-done | bytes 6291472 | tf_op jit(solution)/shard_map/all_gather | solution.py:46
  410.6 6.5 copy.28
  417.1 107.7 %all-to-all-done.2 = bf16[384,8,1024]{2,0,1:T(8,128)(2,1)} async-done(((bf16[384,8,1024]{2,0,1:T(8,128)(2,1)}), bf16[384,8,1024]{2,0,1:T(8,128)(2,1)}, u32[]{:S(2)}, u32[]{:S(2)}) %all-to-all-start.2) | async-done | bytes 6291488 | tf_op jit(solution)/shard_map/all_to_all | solution.py:53
  524.8 4.8 all-to-all-start.3
  529.7 3.3 convert_element_type.54
  533.2 138.3 %all-reduce.3.cloned.1.call-done = f32[160,3072]{1,0:T(8,128)} async-done(((f32[160,3072]{1,0:T(8,128)}), f32[160,3072]{1,0:T(8,128)}) %all-reduce.3.cloned.1.call-update) | async-done | bytes 1966096 | tf_op jit(solution)/shard_map/psum | solution.py:19
  671.5 2.3 fusion.10
  675.5 4.7 fusion.18
  680.1 36.9 %all-gather.17.cloned.1.call-done = bf16[1024,3072]{1,0:T(8,128)(2,1)} async-done(((bf16[1024,768]{1,0:T(8,128)(2,1)}), bf16[1024,3072]{1,0:T(8,128)(2,1)}) %all-gather.17.cloned.1.call-update) | async-done | bytes 6291472 | tf_op jit(solution)/shard_map/all_gather | solution.py:48
  717.1 8.2 fusion.6
  725.3 98.6 %all-reduce.5.cloned.1.call-done = f32[160,3072]{1,0:T(8,128)} async-done(((f32[160,3072]{1,0:T(8,128)}), f32[160,3072]{1,0:T(8,128)}) %all-reduce.5.cloned.1.call-update) | async-done | bytes 1966096 | tf_op jit(solution)/shard_map/psum | solution.py:19
  823.8 2.1 fusion.11
  828.0 6.4 copy.40
  834.4 6.3 copy.41
  840.7 2.7 copy.42
  843.4 6.4 copy.43
  849.8 6.3 copy.44
  856.2 2.7 copy.45
  (60 shorter events, 9.0 us)
Async XLA Ops:
  7.2 55.6 %all-gather.7.cloned.1.call-start = ((), (), s32[]{:S(2)}) async-start(), calls=%async_computation.4 | async-start | bytes 7864320 | tf_op jit(solution)/shard_map/all_gather | solution.py:43
  13.5 97.7 %all-gather.9.cloned.1.call-start = ((), (), s32[]{:S(2)}) async-start(), calls=%async_computation.5 | async-start | bytes 7864320 | tf_op jit(solution)/shard_map/all_gather | solution.py:44
  69.2 5.8 copy-start.6
  69.2 5.9 copy-start.3
  69.2 144.4 %all-to-all-start = ((bf16[384,8,1024]{2,0,1:T(8,128)(2,1)}), bf16[384,8,1024]{2,0,1:T(8,128)(2,1)}, u32[]{:S(2)}, u32[]{:S(2)}) async-start(bf16[384,8,1024]{2,0,1:T(8,128)(2,1)} %bitcast.38), calls=%async_computation | async-start | bytes 12582912 | tf_op jit(solution)/shard_map/all_to_all | solution.py:51
  75.0 145.1 %all-gather.13.cloned.1.call-start = ((), (), s32[]{:S(2)}) async-start(), calls=%async_computation.8 | async-start | bytes 7864320 | tf_op jit(solution)/shard_map/all_gather | solution.py:45
  213.7 5.1 copy-start.4
  213.7 142.7 %all-to-all-start.1 = ((bf16[384,8,1024]{2,0,1:T(8,128)(2,1)}), bf16[384,8,1024]{2,0,1:T(8,128)(2,1)}, u32[]{:S(2)}, u32[]{:S(2)}) async-start(bf16[384,8,1024]{2,0,1:T(8,128)(2,1)} %bitcast.39), calls=%async_computation.1 | async-start | bytes 12582912 | tf_op jit(solution)/shard_map/all_to_all | solution.py:52
  218.7 148.4 %all-gather.11.cloned.1.call-start = ((), (), s32[]{:S(2)}) async-start(), calls=%async_computation.6 | async-start | bytes 7864320 | tf_op jit(solution)/shard_map/all_gather | solution.py:47
  356.4 168.4 %all-to-all-start.2 = ((bf16[384,8,1024]{2,0,1:T(8,128)(2,1)}), bf16[384,8,1024]{2,0,1:T(8,128)(2,1)}, u32[]{:S(2)}, u32[]{:S(2)}) async-start(bf16[384,8,1024]{2,0,1:T(8,128)(2,1)} %bitcast.36), calls=%async_computation.2 | async-start | bytes 12582912 | tf_op jit(solution)/shard_map/all_to_all | solution.py:53
  361.2 1.2 copy-start
  361.2 49.4 %all-gather.15.cloned.1.call-start = ((), (), s32[]{:S(2)}) async-start(), calls=%async_computation.9 | async-start | bytes 7864320 | tf_op jit(solution)/shard_map/all_gather | solution.py:46
  361.8 309.7 %all-reduce.3.cloned.1.call-start = ((), (), s32[]{:S(2)}) async-start(), calls=%async_computation.7 | async-start | bytes 3932160 | tf_op jit(solution)/shard_map/psum | solution.py:19
  524.8 192.3 %all-to-all-start.3 = ((bf16[384,8,1024]{2,0,1:T(8,128)(2,1)}), bf16[384,8,1024]{2,0,1:T(8,128)(2,1)}, u32[]{:S(2)}, u32[]{:S(2)}) async-start(bf16[384,8,1024]{2,0,1:T(8,128)(2,1)} %bitcast.37), calls=%async_computation.3 | async-start | bytes 12582912 | tf_op jit(solution)/shard_map/all_to_all | solution.py:54
  529.6 3.6 copy-start.5
  529.6 187.4 %all-gather.17.cloned.1.call-start = ((), (), s32[]{:S(2)}) async-start(), calls=%async_computation.10 | async-start | bytes 7864320 | tf_op jit(solution)/shard_map/all_gather | solution.py:48
  533.0 290.8 %all-reduce.5.cloned.1.call-start = ((), (), s32[]{:S(2)}) async-start(), calls=%async_computation.11 | async-start | bytes 3932160 | tf_op jit(solution)/shard_map/psum | solution.py:19
  671.5 2.3 copy-start.1
  823.8 2.1 copy-start.2
  828.0 12.7 %slice-start = ((s8[6291456]{0:T(1024)(128)(4,1)}), s8[4194304]{0:T(1024)(128)(4,1)S(1)}, s32[]{:S(2)}) async-start(s8[6291456]{0:T(1024)(128)(4,1)} %bitcast.40), calls=%async_computation.12 | async-start | bytes 8388608
  834.4 6.4 slice-start.1
  843.4 12.7 %slice-start.2 = ((s8[6291456]{0:T(1024)(128)(4,1)}), s8[4194304]{0:T(1024)(128)(4,1)S(1)}, s32[]{:S(2)}) async-start(s8[6291456]{0:T(1024)(128)(4,1)} %bitcast.42), calls=%async_computation.14 | async-start | bytes 8388608
  849.8 6.4 slice-start.3
Sparse Core Ops, SparseCore 0:
  13.6 49.0 all-gather.6
  64.9 46.3 all-gather.8
  113.4 46.3 all-gather.12
  221.3 46.7 all-gather.10
  363.8 46.7 all-gather.14
  414.6 256.8 all-reduce.2
  673.6 43.3 all-gather.16
  725.4 98.3 all-reduce.4
where the time goes:
time: 866 us
  waiting for transfers between devices  723 us (83%)
  local copies, waits for them, and re-layouts  58.3 us (7%)
  matrix products  25.7 us (3%)
  other arithmetic  23.5 us (3%)
  starting transfers between devices  20.9 us (2%)
  between operations  14.3 us (2%)
    psum x2, waiting for transfers between devices, half_step(): block = lax.psum(partial_value, 'fs')  237 us
    all_to_all x1, waiting for transfers between devices, on_device(): lax.all_to_all(widened[1], 'fs', split_axis=1, concat_axis=0, tiled=True)  130 us
    all_to_all x1, waiting for transfers between devices, on_device(): lax.all_to_all(widened[2], 'fs', split_axis=1, concat_axis=0, tiled=True)  108 us
    all_to_all x1, waiting for transfers between devices, on_device(): lax.all_to_all(widened[0], 'fs', split_axis=1, concat_axis=0, tiled=True)  95.9 us
    all_gather x1, waiting for transfers between devices, on_device(): lax.all_gather(fold_gain(gate_first, gain_first), 'tp', axis=1, tiled=True)  48.5 us
    all_gather x1, waiting for transfers between devices, on_device(): lax.all_gather(down_second.astype(jnp.bfloat16), 'tp', axis=1, tiled=True)  36.9 us
    all_gather x1, waiting for transfers between devices, on_device(): lax.all_gather(fold_gain(up_second, gain_second), 'tp', axis=1, tiled=True)  34.6 us
    unnamed x28, local copies, waits for them, and re-layouts  31.5 us
  transfers between devices with their start and end apart: 12, of which 9 were waited for; matrix products, arithmetic and copies ran while one was open for 7% of the time, Pallas kernels for 0%

commit v1 on v0

--- a/solution.py
+++ b/solution.py
@@ -16,7 +16,9 @@
     rising = jnp.dot(normed, w_rising, preferred_element_type=jnp.float32)
     hidden = (jax.nn.silu(gate_part) * rising).astype(jnp.bfloat16)
     partial_value = jnp.dot(hidden, w_down, preferred_element_type=jnp.float32)
-    block = lax.psum(partial_value, "fs")
+    block = partial_value
+    for hop in (1, 2, 4):
+        block = block + lax.ppermute(block, "fs", [(dev, dev ^ hop) for dev in range(8)])
     mixed = 1.6817928 * scales[None, :] * normed.astype(jnp.float32) + 0.5 * block
     return plain_norm(mixed).astype(jnp.bfloat16)
 

time: 866 us -> 1000 us (1.15)
  waiting for transfers between devices: 723 us -> 858 us
    ppermute x0 -> x6, waiting for transfers between devices: none -> 421 us  [half_step(): lax.ppermute(block, 'fs', [(dev, dev ^ hop) for dev in range(8)])]
    psum x2 -> x0, waiting for transfers between devices: 237 us -> none  [half_step(): block = lax.psum(partial_value, 'fs')]
    all_gather x1, waiting for transfers between devices: 36.9 us -> 0.02 us  [on_device(): lax.all_gather(down_second.astype(jnp.bfloat16), 'tp', axis=1, tiled=True)]
    all_gather x1, waiting for transfers between devices: 34.6 us -> 0.02 us  [on_device(): lax.all_gather(fold_gain(up_second, gain_second), 'tp', axis=1, tiled=True)]
    all_to_all x1, waiting for transfers between devices: 108 us -> 129 us  [on_device(): lax.all_to_all(widened[2], 'fs', split_axis=1, concat_axis=0, tiled=True)]
    unnamed x28 -> x26, local copies, waits for them, and re-layouts: 31.5 us -> 32.1 us
  transfers between devices with their start and end apart: 12 -> 16, of which waited for: 9 -> 11; matrix products, arithmetic and copies ran while one was open for 7% -> 5% of each run, Pallas kernels for 0% -> 0%
where the time goes in v1:
time: 1000 us
  waiting for transfers between devices  858 us (86%)
  local copies, waits for them, and re-layouts  58.9 us (6%)
  matrix products  26.2 us (3%)
  starting transfers between devices  23.9 us (2%)
  other arithmetic  19.2 us (2%)
  between operations  14.3 us (1%)
    ppermute x6, waiting for transfers between devices, half_step(): lax.ppermute(block, 'fs', [(dev, dev ^ hop) for dev in range(8)])  421 us
    all_to_all x1, waiting for transfers between devices, on_device(): lax.all_to_all(widened[1], 'fs', split_axis=1, concat_axis=0, tiled=True)  131 us
    all_to_all x1, waiting for transfers between devices, on_device(): lax.all_to_all(widened[2], 'fs', split_axis=1, concat_axis=0, tiled=True)  129 us
    all_to_all x1, waiting for transfers between devices, on_device(): lax.all_to_all(widened[0], 'fs', split_axis=1, concat_axis=0, tiled=True)  95.9 us
    all_gather x1, waiting for transfers between devices, on_device(): lax.all_gather(fold_gain(gate_first, gain_first), 'tp', axis=1, tiled=True)  48.5 us
    unnamed x26, local copies, waits for them, and re-layouts  32.1 us
    all_gather x1, waiting for transfers between devices, on_device(): lax.all_gather(fold_gain(up_first, gain_first), 'tp', axis=1, tiled=True)  31.4 us
  transfers between devices with their start and end apart: 16, of which 11 were waited for; matrix products, arithmetic and copies ran while one was open for 5% of the time, Pallas kernels for 0%

profile of v1, /device:TPU:0, one launch (start us, length us, event | category | flops | bytes accessed | tf_op | source)
XLA Modules:
  0.0 1000.9 jit_solution(2677460739637218908)
XLA Ops:
  8.0 5.5 multiply_convert_fusion.3
  14.3 48.5 %all-gather.7.cloned.1.call-done = bf16[384,8192]{1,0:T(8,128)(2,1)} async-done(((bf16[384,2048]{1,0:T(8,128)(2,1)}), bf16[384,8192]{1,0:T(8,128)(2,1)}) %all-gather.7.cloned.1.call-update) | async-done | bytes 6291472 | tf_op jit(solution)/shard_map/all_gather | solution.py:45
  62.7 6.5 copy.31
  69.2 5.8 all-to-all-start
  75.2 4.7 multiply_convert_fusion
  79.9 31.4 %all-gather.9.cloned.1.call-done = bf16[384,8192]{1,0:T(8,128)(2,1)} async-done(((bf16[384,2048]{1,0:T(8,128)(2,1)}), bf16[384,8192]{1,0:T(8,128)(2,1)}) %all-gather.9.cloned.1.call-update) | async-done | bytes 6291472 | tf_op jit(solution)/shard_map/all_gather | solution.py:46
  111.3 6.5 copy.30
  117.8 95.9 %all-to-all-done = bf16[384,8,1024]{2,0,1:T(8,128)(2,1)} async-done(((bf16[384,8,1024]{2,0,1:T(8,128)(2,1)}), bf16[384,8,1024]{2,0,1:T(8,128)(2,1)}, u32[]{:S(2)}, u32[]{:S(2)}) %all-to-all-start) | async-done | bytes 6291488 | tf_op jit(solution)/shard_map/all_to_all | solution.py:53
  213.7 4.8 all-to-all-start.1
  219.0 6.5 copy.29
  225.5 130.6 %all-to-all-done.1 = bf16[384,8,1024]{2,0,1:T(8,128)(2,1)} async-done(((bf16[384,8,1024]{2,0,1:T(8,128)(2,1)}), bf16[384,8,1024]{2,0,1:T(8,128)(2,1)}, u32[]{:S(2)}, u32[]{:S(2)}) %all-to-all-start.1) | async-done | bytes 6291488 | tf_op jit(solution)/shard_map/all_to_all | solution.py:54
  356.1 5.0 all-to-all-start.2
  362.6 6.5 copy.28
  369.1 129.3 %all-to-all-done.2 = bf16[384,8,1024]{2,0,1:T(8,128)(2,1)} async-done(((bf16[384,8,1024]{2,0,1:T(8,128)(2,1)}), bf16[384,8,1024]{2,0,1:T(8,128)(2,1)}, u32[]{:S(2)}, u32[]{:S(2)}) %all-to-all-start.2) | async-done | bytes 6291488 | tf_op jit(solution)/shard_map/all_to_all | solution.py:55
  498.4 5.0 all-to-all-start.3
  506.8 4.9 fusion.15
  511.7 9.0 fusion.5
  522.5 92.0 %collective-permute-done = f32[160,3072]{1,0:T(8,128)S(1)} collective-permute-done((f32[160,3072]{1,0:T(8,128)S(1)}, f32[160,3072]{1,0:T(8,128)S(1)}, u32[]{:S(2)}, u32[]{:S(2)}) %collective-permute-start) | collective-permute-done | bytes 1966112 | tf_op jit(solution)/shard_map/ppermute | solution.py:21
  614.9 67.9 %collective-permute-done.1 = f32[160,3072]{1,0:T(8,128)S(1)} collective-permute-done((f32[160,3072]{1,0:T(8,128)S(1)}, f32[160,3072]{1,0:T(8,128)S(1)}, u32[]{:S(2)}, u32[]{:S(2)}) %collective-permute-start.1) | collective-permute-done | bytes 1966112 | tf_op jit(solution)/shard_map/ppermute | solution.py:21
  683.5 87.0 %collective-permute-done.2 = f32[160,3072]{1,0:T(8,128)S(1)} collective-permute-done((f32[160,3072]{1,0:T(8,128)S(1)}, f32[160,3072]{1,0:T(8,128)S(1)}, u32[]{:S(2)}, u32[]{:S(2)}) %collective-permute-start.2) | collective-permute-done | bytes 1966112 | tf_op jit(solution)/shard_map/ppermute | solution.py:21
  771.6 4.0 fusion.19
  775.7 8.3 fusion.6
  783.9 45.0 %collective-permute-done.3 = f32[160,3072]{1,0:T(8,128)S(1)} collective-permute-done((f32[160,3072]{1,0:T(8,128)}, f32[160,3072]{1,0:T(8,128)S(1)}, u32[]{:S(2)}, u32[]{:S(2)}) %collective-permute-start.3) | collective-permute-done | bytes 1966112 | tf_op jit(solution)/shard_map/ppermute | solution.py:21
  828.9 1.8 add.70
  830.8 43.9 %collective-permute-done.4 = f32[160,3072]{1,0:T(8,128)S(1)} collective-permute-done((f32[160,3072]{1,0:T(8,128)S(1)}, f32[160,3072]{1,0:T(8,128)S(1)}, u32[]{:S(2)}, u32[]{:S(2)}) %collective-permute-start.4) | collective-permute-done | bytes 1966112 | tf_op jit(solution)/shard_map/ppermute | solution.py:21
  875.4 85.6 %collective-permute-done.5 = f32[160,3072]{1,0:T(8,128)S(1)} collective-permute-done((f32[160,3072]{1,0:T(8,128)S(1)}, f32[160,3072]{1,0:T(8,128)S(1)}, u32[]{:S(2)}, u32[]{:S(2)}) %collective-permute-start.5) | collective-permute-done | bytes 1966112 | tf_op jit(solution)/shard_map/ppermute | solution.py:21
  963.2 6.4 copy.38
  969.6 6.3 copy.39
  976.0 2.7 copy.40
  978.7 6.4 copy.41
  985.0 6.3 copy.42
  991.4 2.7 copy.43
  (67 shorter events, 14.0 us)
Async XLA Ops:
  7.2 55.6 %all-gather.7.cloned.1.call-start = ((), (), s32[]{:S(2)}) async-start(), calls=%async_computation.4 | async-start | bytes 7864320 | tf_op jit(solution)/shard_map/all_gather | solution.py:45
  13.5 97.7 %all-gather.9.cloned.1.call-start = ((), (), s32[]{:S(2)}) async-start(), calls=%async_computation.5 | async-start | bytes 7864320 | tf_op jit(solution)/shard_map/all_gather | solution.py:46
  69.2 5.8 copy-start.5
  69.2 5.9 copy-start.1
  69.2 144.4 %all-to-all-start = ((bf16[384,8,1024]{2,0,1:T(8,128)(2,1)}), bf16[384,8,1024]{2,0,1:T(8,128)(2,1)}, u32[]{:S(2)}, u32[]{:S(2)}) async-start(bf16[384,8,1024]{2,0,1:T(8,128)(2,1)} %bitcast.39), calls=%async_computation | async-start | bytes 12582912 | tf_op jit(solution)/shard_map/all_to_all | solution.py:53
  75.0 144.0 %all-gather.13.cloned.1.call-start = ((), (), s32[]{:S(2)}) async-start(), calls=%async_computation.7 | async-start | bytes 7864320 | tf_op jit(solution)/shard_map/all_gather | solution.py:47
  213.7 142.5 %all-to-all-start.1 = ((bf16[384,8,1024]{2,0,1:T(8,128)(2,1)}), bf16[384,8,1024]{2,0,1:T(8,128)(2,1)}, u32[]{:S(2)}, u32[]{:S(2)}) async-start(bf16[384,8,1024]{2,0,1:T(8,128)(2,1)} %bitcast.40), calls=%async_computation.1 | async-start | bytes 12582912 | tf_op jit(solution)/shard_map/all_to_all | solution.py:54
  218.4 144.2 %all-gather.15.cloned.1.call-start = ((), (), s32[]{:S(2)}) async-start(), calls=%async_computation.8 | async-start | bytes 7864320 | tf_op jit(solution)/shard_map/all_gather | solution.py:48
  356.1 5.1 copy-start.2
  356.1 142.3 %all-to-all-start.2 = ((bf16[384,8,1024]{2,0,1:T(8,128)(2,1)}), bf16[384,8,1024]{2,0,1:T(8,128)(2,1)}, u32[]{:S(2)}, u32[]{:S(2)}) async-start(bf16[384,8,1024]{2,0,1:T(8,128)(2,1)} %bitcast.41), calls=%async_computation.2 | async-start | bytes 12582912 | tf_op jit(solution)/shard_map/all_to_all | solution.py:55
  361.2 150.5 %all-gather.11.cloned.1.call-start = ((), (), s32[]{:S(2)}) async-start(), calls=%async_computation.6 | async-start | bytes 7864320 | tf_op jit(solution)/shard_map/all_gather | solution.py:49
  498.4 5.3 copy-start.3
  498.4 277.3 %all-to-all-start.3 = ((bf16[384,8,1024]{2,0,1:T(8,128)(2,1)}), bf16[384,8,1024]{2,0,1:T(8,128)(2,1)}, u32[]{:S(2)}, u32[]{:S(2)}) async-start(bf16[384,8,1024]{2,0,1:T(8,128)(2,1)} %bitcast.38), calls=%async_computation.3 | async-start | bytes 12582912 | tf_op jit(solution)/shard_map/all_to_all | solution.py:56
  503.4 272.2 %all-gather.17.cloned.1.call-start = ((), (), s32[]{:S(2)}) async-start(), calls=%async_computation.9 | async-start | bytes 7864320 | tf_op jit(solution)/shard_map/all_gather | solution.py:50
  505.0 1.2 copy-start
  520.8 93.8 %collective-permute-start = (f32[160,3072]{1,0:T(8,128)S(1)}, f32[160,3072]{1,0:T(8,128)S(1)}, u32[]{:S(2)}, u32[]{:S(2)}) collective-permute-start(f32[160,3072]{1,0:T(8,128)S(1)} %fusion.5), channel_id=1, source_target_pairs={{0,4},{4,0},{8,12},{12,8},{16,20},{20,16},{24,28},{28,24},{1,5},{5... | collective-permute-start | bytes 5898248 | tf_op jit(solution)/shard_map/ppermute | solution.py:21
  614.8 68.8 %copy-start.4 = (f32[3072]{0:T(1024)S(1)}, f32[3072]{0:T(1024)}, u32[]{:S(2)}) copy-start(f32[3072]{0:T(1024)} %param.10) | copy-start | bytes 36868
  614.8 68.0 %collective-permute-start.1 = (f32[160,3072]{1,0:T(8,128)S(1)}, f32[160,3072]{1,0:T(8,128)S(1)}, u32[]{:S(2)}, u32[]{:S(2)}) collective-permute-start(f32[160,3072]{1,0:T(8,128)S(1)} %add.64), channel_id=1, source_target_pairs={{0,8},{4,12},{8,0},{12,4},{16,24},{20,28},{24,16},{28,20},{1,9},{5... | collective-permute-start | bytes 5898248 | tf_op jit(solution)/shard_map/ppermute | solution.py:21
  683.0 87.6 %collective-permute-start.2 = (f32[160,3072]{1,0:T(8,128)S(1)}, f32[160,3072]{1,0:T(8,128)S(1)}, u32[]{:S(2)}, u32[]{:S(2)}) collective-permute-start(f32[160,3072]{1,0:T(8,128)S(1)} %add.65), channel_id=1, source_target_pairs={{0,16},{4,20},{8,24},{12,28},{16,0},{20,4},{24,8},{28,12},{1,17},{... | collective-permute-start | bytes 5898248 | tf_op jit(solution)/shard_map/ppermute | solution.py:21
  783.9 45.0 %collective-permute-start.3 = (f32[160,3072]{1,0:T(8,128)}, f32[160,3072]{1,0:T(8,128)S(1)}, u32[]{:S(2)}, u32[]{:S(2)}) collective-permute-start(f32[160,3072]{1,0:T(8,128)} %fusion.6), channel_id=1, source_target_pairs={{0,4},{4,0},{8,12},{12,8},{16,20},{20,16},{24,28},{28,24},{1,5},{5... | collective-permute-start | bytes 5898248 | tf_op jit(solution)/shard_map/ppermute | solution.py:21
  830.7 44.0 %collective-permute-start.4 = (f32[160,3072]{1,0:T(8,128)S(1)}, f32[160,3072]{1,0:T(8,128)S(1)}, u32[]{:S(2)}, u32[]{:S(2)}) collective-permute-start(f32[160,3072]{1,0:T(8,128)S(1)} %add.70), channel_id=1, source_target_pairs={{0,8},{4,12},{8,0},{12,4},{16,24},{20,28},{24,16},{28,20},{1,9},{5... | collective-permute-start | bytes 5898248 | tf_op jit(solution)/shard_map/ppermute | solution.py:21
  874.9 86.1 %collective-permute-start.5 = (f32[160,3072]{1,0:T(8,128)S(1)}, f32[160,3072]{1,0:T(8,128)S(1)}, u32[]{:S(2)}, u32[]{:S(2)}) collective-permute-start(f32[160,3072]{1,0:T(8,128)S(1)} %add.71), channel_id=1, source_target_pairs={{0,16},{4,20},{8,24},{12,28},{16,0},{20,4},{24,8},{28,12},{1,17},{... | collective-permute-start | bytes 5898248 | tf_op jit(solution)/shard_map/ppermute | solution.py:21
  963.2 12.7 %slice-start.2 = ((s8[6291456]{0:T(1024)(128)(4,1)}), s8[4194304]{0:T(1024)(128)(4,1)S(1)}, s32[]{:S(2)}) async-start(s8[6291456]{0:T(1024)(128)(4,1)} %bitcast.42), calls=%async_computation.12 | async-start | bytes 8388608
  969.6 6.4 slice-start.3
  978.7 12.7 %slice-start = ((s8[6291456]{0:T(1024)(128)(4,1)}), s8[4194304]{0:T(1024)(128)(4,1)S(1)}, s32[]{:S(2)}) async-start(s8[6291456]{0:T(1024)(128)(4,1)} %bitcast.36), calls=%async_computation.10 | async-start | bytes 8388608
  985.0 6.4 slice-start.1
Sparse Core Ops, SparseCore 0:
  13.6 49.0 all-gather.6
  64.9 46.3 all-gather.8
  113.4 46.3 all-gather.12
  221.1 46.7 all-gather.14
  363.8 46.7 all-gather.10
  506.1 46.7 all-gather.16
